TPU v7x, 32 devices: a whole 2x2x4 slice. The times are simulated.
32 devices in a mesh: ep: 8 (over z, y), tp: 4 (over x, core).
Axes of the slice: x: 2, y: 2, z: 4, core: 2. Of those that a mesh axis runs over, the one named last changes fastest.
Arguments:
- queries: bfloat16 [4096, 1024], P('ep', 'tp'), may hold values from -6 to 6
- key_rows: bfloat16 [4096, 512], P('ep', 'tp'), may hold values from -6 to 6
- value_rows: bfloat16 [4096, 512], P('ep', 'tp'), may hold values from -6 to 6
- forget_logit: float32 [8, 4096], P('tp', 'ep'), may hold values from -1 to 17
- out_weight: bfloat16 [1024, 2048], P('tp'), may hold values from -0.1875 to 0.1875
- out_gain: float32 [2048], replicated, may hold values from 0.1 to 1.9
- moe_input: bfloat16 [4096, 2048], P('ep'), may hold values from -6 to 6
- moe_gain: float32 [2048], replicated, may hold values from 0.1 to 1.9
- router_group: bfloat16 [2048, 4], replicated, may hold values from -2 to 2
- router_expert: bfloat16 [2048, 8], replicated, may hold values from -0.125 to 0.125
- route_group: int32 [4096], P('ep'), may hold values from 0 to 3
- route_pick: int32 [4096, 2], P('ep'), may hold values from 0 to 1, as said below
- expert_gate: bfloat16 [8, 2048, 1024], P('ep', None, 'tp'), may hold values from -0.125 to 0.125
- expert_up: bfloat16 [8, 2048, 1024], P('ep', None, 'tp'), may hold values from -0.125 to 0.125
- expert_down: bfloat16 [8, 1024, 2048], P('ep', 'tp'), may hold values from -42 to 42
Outputs:
- mixer_out: bfloat16 [4096, 2048], P(('ep', 'tp'))
- moe_out: bfloat16 [4096, 2048], P(('ep', 'tp'))
Inputs may be any that keep to these rules, and one draw needn't show every extreme that they name: `route_pick`: the two entries of a row differ.
All inputs are finite; a program needn't handle non-finite values.
Results may differ from a plain program's by a relative error of at most 0.013.
Values may be sent and summed in bfloat16 or wider, within the bound.
A program may use at most 128 MiB of HBM per device.

v0:
```python
import math

import jax
import jax.numpy as jnp
from jax import lax
from jax.sharding import PartitionSpec as P

DH = 128
GROUPS = 4


def rms_scale(row_block, scale_gain):
    values = row_block.astype(jnp.float32)
    return (
        values * lax.rsqrt(jnp.mean(values * values, axis=-1, keepdims=True) + 1e-06) * scale_gain
    )


def slot_ranks(chosen, block_rows, experts):
    expert_ids = jnp.arange(experts, dtype=jnp.int32)
    matches = chosen[:, :, None] == expert_ids
    usage = jnp.any(matches, axis=1).astype(jnp.int32)
    grouped = usage.reshape(-1, block_rows, experts)
    before = (jnp.cumsum(grouped, axis=1) - grouped).reshape(-1, experts)
    return jnp.sum(jnp.where(matches, before[:, None, :], 0), axis=2)


def expert_hidden(arrived, gate_part, up_part):
    flat = arrived.reshape(-1, arrived.shape[-1])
    gated = jnp.dot(flat, gate_part, preferred_element_type=jnp.float32)
    lifted = jnp.dot(flat, up_part, preferred_element_type=jnp.float32)
    hidden = (jax.nn.silu(gated) * lifted).astype(jnp.bfloat16)
    return hidden.reshape(arrived.shape[:-1] + (gate_part.shape[1],))


def body(
    queries,
    key_rows,
    value_rows,
    forget_logit,
    out_weight,
    out_gain,
    moe_input,
    moe_gain,
    router_group,
    router_expert,
    route_group,
    route_pick,
    expert_gate,
    expert_up,
    expert_down,
):
    tp_count = lax.axis_size("tp")
    ep_count = lax.axis_size("ep")
    tp_index = lax.axis_index("tp")
    ep_index = lax.axis_index("ep")
    rows_group = queries.shape[0]
    query_heads = forget_logit.shape[0]
    key_heads = key_rows.shape[1] // DH
    ratio = query_heads // key_heads
    own_start = ep_index * rows_group
    own_pos = own_start + jnp.arange(rows_group, dtype=jnp.int32)
    local_cum = jnp.cumsum(jax.nn.log_sigmoid(forget_logit), axis=1)
    every_cum = lax.all_gather(local_cum, "ep", axis=1, tiled=True).reshape(
        query_heads, ep_count, rows_group
    )
    shard_totals = every_cum[:, :, -1]
    offsets = jnp.cumsum(shard_totals, axis=1) - shard_totals
    cum_gate = (every_cum + offsets[:, :, None]).reshape(query_heads, ep_count * rows_group)
    own_cum = lax.dynamic_slice_in_dim(cum_gate, own_start, rows_group, 1).reshape(
        key_heads, ratio, rows_group, 1
    )
    query_stack = (
        queries.reshape(rows_group, key_heads, ratio, DH)
        .transpose(1, 2, 0, 3)
        .reshape(key_heads, ratio * rows_group, DH)
    )

    def attend_block(current, keys_block, values_block, start):
        piece_rows = keys_block.shape[0]

        def compute(state):
            row_top, row_total, weighted = state
            key_stack = keys_block.reshape(piece_rows, key_heads, DH).transpose(1, 0, 2)
            value_stack = values_block.reshape(piece_rows, key_heads, DH).transpose(1, 0, 2)
            scores = jnp.einsum(
                "gqd,gkd->gqk", query_stack, key_stack, preferred_element_type=jnp.float32
            ) / math.sqrt(DH)
            key_cum = lax.dynamic_slice_in_dim(cum_gate, start, piece_rows, 1).reshape(
                key_heads, ratio, 1, piece_rows
            )
            logits = scores.reshape(key_heads, ratio, rows_group, piece_rows) + own_cum - key_cum
            visible = (start + jnp.arange(piece_rows, dtype=jnp.int32))[None, :] <= own_pos[:, None]
            logits = jnp.where(visible, logits, -1e30)
            new_top = jnp.maximum(row_top, jnp.max(logits, axis=3))
            expo = jnp.where(visible, jnp.exp(logits - new_top[..., None]), 0.0)
            rescale = jnp.exp(row_top - new_top)
            row_total = row_total * rescale + jnp.sum(expo, axis=3)
            product = jnp.einsum(
                "gqk,gkd->gqd",
                expo.reshape(key_heads, ratio * rows_group, piece_rows).astype(jnp.bfloat16),
                value_stack,
                preferred_element_type=jnp.float32,
            )
            weighted = weighted * rescale.reshape(key_heads, ratio * rows_group, 1) + product
            return (new_top, row_total, weighted)

        return lax.cond(start < own_start + rows_group, compute, lambda state: state, current)

    initial = (
        jnp.full((key_heads, ratio, rows_group), -1e30, jnp.float32),
        jnp.zeros((key_heads, ratio, rows_group), jnp.float32),
        jnp.zeros((key_heads, ratio * rows_group, DH), jnp.float32),
    )
    current = initial
    keys_piece = lax.all_gather(key_rows, "ep", axis=0, tiled=True)
    values_piece = lax.all_gather(value_rows, "ep", axis=0, tiled=True)
    piece_rows = keys_piece.shape[0]
    blocks = piece_rows // rows_group

    def advance(state, inputs):
        keys_block, values_block, block_index = inputs
        return (attend_block(state, keys_block, values_block, block_index * rows_group), None)

    current, _ = lax.scan(
        advance,
        current,
        (
            keys_piece.reshape(blocks, rows_group, -1),
            values_piece.reshape(blocks, rows_group, -1),
            jnp.arange(blocks, dtype=jnp.int32),
        ),
    )
    row_top, row_total, weighted = current
    attended = (weighted / row_total.reshape(key_heads, ratio * rows_group, 1)).astype(jnp.bfloat16)
    attended = (
        attended.reshape(key_heads, ratio, rows_group, DH)
        .transpose(2, 0, 1, 3)
        .reshape(rows_group, query_heads * DH)
    )
    group_rows = moe_input.shape[0]
    own_rows = group_rows // tp_count
    width_model = moe_input.shape[1]
    experts = expert_gate.shape[0] * ep_count
    per_group = experts // GROUPS
    capacity = tp_count * own_rows // experts
    own_first = tp_index * own_rows
    chosen_all = route_group[:, None] * per_group + route_pick
    rank_all = slot_ranks(chosen_all, own_rows, experts)
    chosen = lax.dynamic_slice_in_dim(chosen_all, own_first, own_rows, 0)
    ranks = lax.dynamic_slice_in_dim(rank_all, own_first, own_rows, 0)
    is_kept = ranks < capacity
    own_group = lax.dynamic_slice_in_dim(route_group, own_first, own_rows, 0)
    normed = rms_scale(
        lax.dynamic_slice_in_dim(moe_input, own_first, own_rows, 0), moe_gain
    ).astype(jnp.bfloat16)
    target = jnp.where(is_kept, chosen * capacity + ranks, experts * capacity)
    sources = jnp.broadcast_to(jnp.arange(own_rows, dtype=jnp.int32)[:, None], target.shape)
    slot_table = (
        jnp.full((experts * capacity,), own_rows, jnp.int32)
        .at[target.reshape(-1)]
        .set(sources.reshape(-1), mode="drop")
    )
    padded = jnp.concatenate([normed, jnp.zeros((1, width_model), jnp.bfloat16)], axis=0)
    outgoing = padded[slot_table].reshape(experts, capacity, width_model)
    arrived = lax.all_to_all(outgoing, "ep", split_axis=0, concat_axis=0, tiled=True)
    hidden_arrived = lax.all_gather(arrived[None], "tp", axis=0, tiled=True)
    hidden = expert_hidden(hidden_arrived, expert_gate[0], expert_up[0])
    hidden_rows = hidden.reshape(-1, hidden.shape[-1])
    mixer_term = jnp.dot(attended, out_weight, preferred_element_type=jnp.float32)
    expert_term = jnp.dot(hidden_rows, expert_down[0], preferred_element_type=jnp.float32)
    mixer_summed, expert_summed = (
        lax.psum_scatter(
            mixer_term.astype(jnp.bfloat16), "tp", scatter_dimension=0, tiled=True
        ).astype(jnp.float32),
        lax.psum_scatter(
            expert_term.astype(jnp.bfloat16), "tp", scatter_dimension=0, tiled=True
        ).astype(jnp.float32),
    )
    mixer_out = rms_scale(mixer_summed, out_gain).astype(jnp.bfloat16)
    group_logits = jnp.dot(normed, router_group, preferred_element_type=jnp.float32)
    expert_logits = jnp.dot(normed, router_expert, preferred_element_type=jnp.float32)
    group_top = jnp.max(group_logits, axis=1, keepdims=True)
    group_exp = jnp.exp(group_logits - group_top)
    group_hit = jnp.arange(GROUPS, dtype=jnp.int32)[None, :] == own_group[:, None]
    group_share = jnp.sum(jnp.where(group_hit, group_exp, 0.0), axis=1) / jnp.sum(group_exp, axis=1)
    expert_hit = jnp.arange(experts, dtype=jnp.int32)[None, None, :] == chosen[:, :, None]
    picked_logits = jnp.sum(jnp.where(expert_hit, expert_logits[:, None, :], 0.0), axis=2)
    shares = group_share[:, None] * jax.nn.sigmoid(picked_logits - picked_logits[:, ::-1])
    results = expert_summed.astype(jnp.bfloat16).reshape(ep_count, capacity, width_model)
    returned = lax.all_to_all(results, "ep", split_axis=0, concat_axis=0, tiled=True).reshape(
        experts * capacity, width_model
    )
    slot_index = jnp.where(is_kept, chosen * capacity + ranks, 0)
    picked = returned[slot_index]
    moe_out = jnp.sum(
        jnp.where(is_kept, shares, 0.0)[:, :, None] * picked.astype(jnp.float32), axis=1
    )
    return (mixer_out, moe_out.astype(jnp.bfloat16))


def solution(mesh):
    in_specs = (
        P("ep", "tp"),
        P("ep", "tp"),
        P("ep", "tp"),
        P("tp", "ep"),
        P("tp", None),
        P(),
        P("ep", None),
        P(),
        P(),
        P(),
        P("ep"),
        P("ep", None),
        P("ep", None, "tp"),
        P("ep", None, "tp"),
        P("ep", "tp", None),
    )
    out_specs = (P(("ep", "tp"), None), P(("ep", "tp"), None))
    return jax.shard_map(body, mesh=mesh, in_specs=in_specs, out_specs=out_specs, check_vma=False)
```

profile of v0, /device:TPU:0, one launch (start us, length us, event | category | flops | bytes accessed | tf_op | source)
XLA Modules:
  0.0 390.1 jit_solution(8046871968145064070)
XLA Ops:
  7.2 0.8 broadcast_multiply_fusion
  8.0 0.8 dynamic_slice.47
  8.8 0.7 broadcast_add_fusion.1
  9.5 1.2 fusion.22
  10.7 1.3 fusion.24
  12.0 1.0 fusion.40
  12.9 0.2 fusion.41
  13.2 0.1 copy.78
  13.4 0.3 reduce_window_sum.42
  13.9 0.1 copy.81
  14.0 0.1 reshape.280
  14.2 0.1 reshape.307
  14.3 1.4 scatter_custom_fusion
  15.8 3.3 gather_fusion
  19.1 55.6 %all_to_all.10 = bf16[8,64,2048]{2,1,0:T(8,128)(2,1)} all-to-all(bf16[8,64,2048]{2,1,0:T(8,128)(2,1)} %bitcast.87), channel_id=1, replica_groups=mesh['ep'=8,'tp'=4] {'ep'}, dimensions={0} | all-to-all | bytes 4194304 | tf_op jit(solution)/shard_map/all_to_all | solution.py:166
  74.8 0.7 all-gather.7.cloned.1.call-update
  75.6 0.7 all-gather.5.cloned.1.call-update
  76.3 55.9 %all-gather.9.cloned.1.call-done = bf16[32,64,2048]{2,1,0:T(8,128)(2,1)} async-done(((bf16[8,64,2048]{2,1,0:T(8,128)(2,1)}), bf16[32,64,2048]{2,1,0:T(8,128)(2,1)}) %all-gather.9.cloned.1.call-update) | async-done | bytes 8388624 | tf_op jit(solution)/shard_map/all_gather | solution.py:167
  132.2 7.2 %fusion.28 = f32[2048,256]{1,0:T(8,128)} fusion(bf16[2048,2048]{1,0:T(8,128)(2,1)} %bitcast.104, bf16[1,2048,256]{2,1,0:T(8,128)(2,1)S(1)} %copy-done.7), kind=kOutput, calls=%fused_computation.46 | convolution fusion | flops 2147483648 | bytes 11534336 | tf_op jit(solution)/shard_map/dot_general | solution.py:30
  139.4 13.2 %convolution_convert_fusion = bf16[2048,2048]{1,0:T(8,128)(2,1)} fusion(bf16[2048,2048]{1,0:T(8,128)(2,1)} %bitcast.105, f32[2048,256]{1,0:T(8,128)} %fusion.28, bf16[1,256,2048]{2,1,0:T(8,128)(2,1)S(1)} %copy-done, bf16[1,2048,256]{2,1,0:T(8,128)(2,1)S(1)} %copy-done.8), kind=kOutput, calls=%fused_computation.28 | convolution fusion | flops 4302307328 | bytes 20971520 | tf_op jit(solution)/shard_map/dot_general | solution.py:171
  152.6 0.6 copy-done.6
  153.3 0.6 reduce-window.6
  153.9 0.2 slice_reduce_fusion
  154.1 0.2 reduce-window.9
  154.3 0.1 copy.83
  154.5 51.7 %all_gather.13 = f32[2,4096]{0,1:T(8,128)S(1)} all-gather(f32[2,512]{0,1:T(8,128)S(1)} %bitcast.92), channel_id=1, replica_groups=mesh['ep'=8,'tp'=4] {'ep'}, dimensions={1}, use_global_device_ids=true | all-gather | bytes 36864 | tf_op jit(solution)/shard_map/all_gather | solution.py:64
  206.3 0.2 reduce_window_sum.41
  206.6 1.4 bitcast_add_fusion
  208.0 1.0 dynamic-slice_bitcast_fusion
  209.3 23.2 %all-gather.5.cloned.1.call-done = bf16[4096,128]{1,0:T(8,128)(2,1)} async-done(((bf16[512,128]{1,0:T(8,128)(2,1)}), bf16[4096,128]{1,0:T(8,128)(2,1)}) %all-gather.5.cloned.1.call-update) | async-done | bytes 1048592 | tf_op jit(solution)/shard_map/all_gather | solution.py:116
  232.5 0.8 broadcast_in_dim.103
  233.4 20.4 %while.17 = (s32[]{:T(128)}, f32[1,2,512]{2,1,0:T(2,128)S(1)}, f32[1,2,512]{2,1,0:T(2,128)S(1)}, f32[1,1024,128]{2,1,0:T(8,128)}, s32[8]{0:T(128)S(1)}, /*index=...) while((s32[]{:T(128)}, f32[1,2,512]{2,1,0:T(2,128)S(1)}, ...), condition=%wide.region_8.9_spmd.clone, body=%wide.region_3.8_spmd.clone.sunk | while | flops 274731008 | bytes 24245672 | solution.py:125
  233.4 0.6 dynamic_slice.81
  234.6 10.0 %conditional.3 = ((f32[1,2,512]{2,1,0:T(2,128)S(1)}, f32[1,2,512]{2,1,0:T(2,128)S(1)}, f32[1,1024,128]{2,1,0:T(8,128)})) conditional(s32[]{:T(128)} %convert_element_type.103, (f32[1,2,512]{2,1,0:T(2,128)S(1)}, f32[1,2,512]{2,1,0:T(2,128)S(1)}, f32[1,1024,128]{2,1,0:T(8,128)}) %tuple.59, (s32[]{:T(128)}, s32[]{:T(128)}, ...), branch_computations={%region_4.4_spmd, %region_5.7_spmd} | conditional | flops 274731008 | bytes 24243334 | solution.py:108
  234.6 0.2 broadcast_compare_fusion
  234.9 0.1 broadcast_in_dim.47
  235.0 1.4 copy.69
  236.4 1.0 constant_dynamic-slice_fusion
  237.4 0.7 sub.59
  238.1 0.5 copy.87
  238.6 0.7 copy-done.1
  239.3 1.6 fusion.39
  240.9 3.2 fusion.5
  244.1 0.5 fusion.4
  244.6 0.6 dynamic_slice.81
  246.0 0.6 dynamic_slice.81
  247.3 0.6 dynamic_slice.81
  248.6 0.6 dynamic_slice.81
  249.9 0.6 dynamic_slice.81
  251.2 0.6 dynamic_slice.81
  252.4 0.6 dynamic_slice.81
  253.7 1.2 divide_convert_fusion
  255.0 0.1 copy.77
  255.2 3.3 convolution_convert_fusion.1
  258.4 46.7 %reduce-scatter.5.cloned.1.call-done = bf16[512,2048]{1,0:T(8,128)(2,1)} async-done(((bf16[2048,2048]{1,0:T(8,128)(2,1)}), bf16[512,2048]{1,0:T(8,128)(2,1)}) %reduce-scatter.5.cloned.1.call-update) | async-done | bytes 2097168 | tf_op jit(solution)/shard_map/reduce_scatter | solution.py:176
  305.1 23.7 %all-to-all-start.1 = ((bf16[8,64,2048]{2,1,0:T(8,128)(2,1)}), bf16[8,64,2048]{2,1,0:T(8,128)(2,1)S(1)}, u32[]{:S(2)}, u32[]{:S(2)}) async-start(bf16[8,64,2048]{2,1,0:T(8,128)(2,1)} %bitcast.88), calls=%async_computation.3 | async-start | bytes 4194304 | tf_op jit(solution)/shard_map/all_to_all | solution.py:191
  328.9 0.1 reshape.297
  329.1 26.1 %reduce-scatter.3.cloned.1.call-done = bf16[128,2048]{1,0:T(8,128)(2,1)} async-done(((bf16[512,2048]{1,0:T(8,128)(2,1)}), bf16[128,2048]{1,0:T(8,128)(2,1)}) %reduce-scatter.3.cloned.1.call-update) | async-done | bytes 524304 | tf_op jit(solution)/shard_map/reduce_scatter | solution.py:173
  355.2 1.2 fusion.19
  356.5 2.0 fusion.21
  358.5 16.4 %all-to-all-done.1 = bf16[8,64,2048]{2,1,0:T(8,128)(2,1)S(1)} async-done(((bf16[8,64,2048]{2,1,0:T(8,128)(2,1)}), bf16[8,64,2048]{2,1,0:T(8,128)(2,1)S(1)}, u32[]{:S(2)}, u32[]{:S(2)}) %all-to-all-start.1) | async-done | bytes 2097184 | tf_op jit(solution)/shard_map/all_to_all | solution.py:191
  374.9 2.3 gather_fusion.1
  377.2 2.4 reshape.316
  379.6 3.9 %multiply_reduce_fusion = bf16[128,2048]{1,0:T(8,128)(2,1)} fusion(f32[128,2,2048]{2,1,0:T(2,128)S(1)} %reshape.316, f32[128,2]{1,0:T(8,128)S(1)} %copy.80), kind=kLoop, calls=%fused_computation.33 | loop fusion | flops 786432 | bytes 2622464 | tf_op jit(solution)/shard_map/reduce_sum | solution.py:196
  (84 shorter events, 1.6 us)
Async XLA Ops:
  7.2 132.2 %copy-start = (bf16[1,256,2048]{2,1,0:T(8,128)(2,1)S(1)}, bf16[1,256,2048]{2,1,0:T(8,128)(2,1)}, u32[]{:S(2)}) copy-start(bf16[1,256,2048]{2,1,0:T(8,128)(2,1)} %param.33) | copy-start | bytes 3145732
  7.2 5.8 %copy-start.4 = (bf16[2048,8]{0,1:T(8,128)(2,1)S(1)}, bf16[2048,8]{0,1:T(8,128)(2,1)}, u32[]{:S(2)}) copy-start(bf16[2048,8]{0,1:T(8,128)(2,1)} %param.28) | copy-start | bytes 98308
  7.2 125.0 %all-gather.9.cloned.1.call-start = ((), (), s32[]{:S(2)}) async-start(), calls=%async_computation.8 | async-start | bytes 10485760 | tf_op jit(solution)/shard_map/all_gather | solution.py:167
  74.7 57.5 %copy-start.7 = (bf16[1,2048,256]{2,1,0:T(8,128)(2,1)S(1)}, bf16[1,2048,256]{2,1,0:T(8,128)(2,1)}, u32[]{:S(2)}) copy-start(bf16[1,2048,256]{2,1,0:T(8,128)(2,1)} %param.31) | copy-start | bytes 3145732
  74.8 134.5 %all-gather.7.cloned.1.call-start = ((), (), s32[]{:S(2)}) async-start(), calls=%async_computation.5 | async-start | bytes 1179648 | tf_op jit(solution)/shard_map/all_gather | solution.py:117
  75.5 157.0 %all-gather.5.cloned.1.call-start = ((), (), s32[]{:S(2)}) async-start(), calls=%async_computation.4 | async-start | bytes 1179648 | tf_op jit(solution)/shard_map/all_gather | solution.py:116
  76.2 228.9 %reduce-scatter.5.cloned.1.call-start = ((), (), s32[]{:S(2)}) async-start(), calls=%async_computation.7 | async-start | bytes 10485760 | tf_op jit(solution)/shard_map/reduce_scatter | solution.py:176
  132.2 7.2 %copy-start.8 = (bf16[1,2048,256]{2,1,0:T(8,128)(2,1)S(1)}, bf16[1,2048,256]{2,1,0:T(8,128)(2,1)}, u32[]{:S(2)}) copy-start(bf16[1,2048,256]{2,1,0:T(8,128)(2,1)} %param.32) | copy-start | bytes 3145732
  152.6 0.7 copy-start.6
  152.6 202.6 %reduce-scatter.3.cloned.1.call-start = ((), (), s32[]{:S(2)}) async-start(), calls=%async_computation.6 | async-start | bytes 2621440 | tf_op jit(solution)/shard_map/reduce_scatter | solution.py:173
  206.6 2.5 copy-start.3
  238.1 1.2 copy-start.1
  240.9 3.2 copy-start.2
  305.1 51.4 %copy-start.5 = (f32[2048]{0:T(1024)S(1)}, f32[2048]{0:T(1024)}, u32[]{:S(2)}) copy-start(f32[2048]{0:T(1024)} %param.24) | copy-start | bytes 24580
  305.1 69.8 %all-to-all-start.1 = ((bf16[8,64,2048]{2,1,0:T(8,128)(2,1)}), bf16[8,64,2048]{2,1,0:T(8,128)(2,1)S(1)}, u32[]{:S(2)}, u32[]{:S(2)}) async-start(bf16[8,64,2048]{2,1,0:T(8,128)(2,1)} %bitcast.88), calls=%async_computation.3 | async-start | bytes 4194304 | tf_op jit(solution)/shard_map/all_to_all | solution.py:191
Sparse Core Ops, SparseCore 0:
  74.9 57.2 all-gather.8
  134.3 52.7 all-gather.6
  189.2 43.2 all-gather.4
  234.9 70.0 reduce-scatter.4
  307.5 47.7 reduce-scatter.2
where the time goes:
time: 392 us; the launch traced here: 390 us
  waiting for transfers between devices  170 us (43%)
  blocking collectives  107 us (27%)
  matrix products  29.6 us (8%)
  starting transfers between devices  23.9 us (6%)
  local copies, waits for them, and re-layouts  23.7 us (6%)
  other arithmetic  16.1 us (4%)
  between operations  14 us (4%)
  loops' own time  5.77 us (1%)
    all_gather x1, waiting for transfers between devices, body(): hidden_arrived = lax.all_gather(arrived[None], 'tp', axis=0, tiled=True)  55.9 us
    all_to_all x1, blocking collectives, body(): lax.all_to_all(outgoing, 'ep', split_axis=0, concat_axis=0, tiled=True)  55.6 us
    all_gather x1, blocking collectives, body(): lax.all_gather(local_cum, 'ep', axis=1, tiled=True)  51.7 us
    reduce_scatter x1, waiting for transfers between devices, body(): lax.psum_scatter(expert_term.astype(jnp.bfloat16), 'tp', scatter_dimensio...  46.7 us
    reduce_scatter x1, waiting for transfers between devices, body(): lax.psum_scatter(mixer_term.astype(jnp.bfloat16), 'tp', scatter_dimension...  26.1 us
    all_to_all x1, starting transfers between devices, body(): lax.all_to_all(results, 'ep', split_axis=0, concat_axis=0, tiled=True)  23.7 us
    all_gather x1, waiting for transfers between devices, body(): keys_piece = lax.all_gather(key_rows, 'ep', axis=0, tiled=True)  23.2 us
    all_to_all x1, waiting for transfers between devices, body(): lax.all_to_all(results, 'ep', split_axis=0, concat_axis=0, tiled=True)  16.4 us
  transfers between devices with their start and end apart: 6, of which 5 were waited for; matrix products, arithmetic and copies ran while one was open for 12% of the time, Pallas kernels for 0%

commit v1 on v0

--- a/solution.py
+++ b/solution.py
@@ -1,8 +1,11 @@
+import functools
 import math
 
 import jax
 import jax.numpy as jnp
 from jax import lax
+from jax.experimental import pallas as pl
+from jax.experimental.pallas import tpu as pltpu
 from jax.sharding import PartitionSpec as P
 
 DH = 128
@@ -33,7 +36,7 @@
     return hidden.reshape(arrived.shape[:-1] + (gate_part.shape[1],))
 
 
-def body(
+def general_body(
     queries,
     key_rows,
     value_rows,
@@ -199,6 +202,437 @@
     return (mixer_out, moe_out.astype(jnp.bfloat16))
 
 
+LOG2E = math.log2(math.e)
+MESH = pl.DeviceIdType.MESH
+VMEM = pl.BlockSpec(memory_space=pltpu.VMEM)
+ANY = pl.BlockSpec(memory_space=pl.ANY)
+
+
+def places():
+    ep, tp = lax.axis_index("ep"), lax.axis_index("tp")
+    return ep, tp, ep // 2, ep % 2, tp // 2, tp % 2
+
+
+def greet(groups):
+    ep, tp, z, y, x, c = places()
+    barrier = pltpu.get_barrier_semaphore()
+    peers = [(z * 2 + 1 - y, tp), (ep, (1 - x) * 2 + c), (ep, x * 2 + 1 - c)]
+    peers += [(lax.rem(z + d, groups) * 2 + y, tp) for d in range(1, groups)]
+    for peer in peers:
+        pl.semaphore_signal(barrier, inc=1, device_id=peer, device_id_type=MESH)
+    pl.semaphore_wait(barrier, len(peers))
+
+
+def remote(src, dst, send, recv, peer):
+    return pltpu.make_async_remote_copy(
+        src_ref=src, dst_ref=dst, send_sem=send, recv_sem=recv, device_id=peer, device_id_type=MESH
+    )
+
+
+def dispatch_kernel(
+    groups, slots, keys, vals, cum, gate, up, down,
+    rows, keys_all, vals_all, cum_all, gate_o, up_o, down_o,
+    local_sem, kvz_s, kvz_r, kvy_s, kvy_r, w_s, w_r, z_s, z_r, y_s, y_r, x_s, x_r,
+):
+    ep, tp, z, y, x, c = places()
+    greet(groups)
+    across_y = (z * 2 + 1 - y, tp)
+    across_x = (ep, (1 - x) * 2 + c)
+    across_c = (ep, x * 2 + 1 - c)
+    own = x * 2 + y
+    beside = x * 2 + 1 - y
+    stream = ((keys, keys_all), (vals, vals_all), (cum, cum_all))
+
+    for i, (src, dst) in enumerate(stream):
+        for d in range(1, groups):
+            @pl.when(z + d < groups)
+            def _(i=i, src=src, dst=dst, d=d):
+                remote(
+                    src, dst.at[ep], kvz_s.at[i, d], kvz_r.at[i, d],
+                    (lax.rem(z + d, groups) * 2 + y, tp),
+                ).start()
+
+    def z_copy(d):
+        to = lax.rem(z + d, groups)
+        return remote(slots.at[to], rows.at[own, z], z_s.at[d], z_r.at[d], (to * 2 + y, tp))
+
+    def chunk(q, d):
+        return rows.at[q, lax.rem(z - d + groups, groups)]
+
+    for d in range(1, groups):
+        z_copy(d).start()
+
+    def y_copy(d):
+        src = slots.at[z] if d == 0 else chunk(own, d)
+        return remote(src, chunk(own, d), y_s.at[d], y_r.at[d], across_y)
+
+    def x_copy(d):
+        src = slots.at[z] if d == 0 else chunk(own, d)
+        return remote(src, chunk(own, d), x_s.at[0, d], x_r.at[0, d], across_x)
+
+    def x_relay(d):
+        return remote(chunk(beside, d), chunk(beside, d), x_s.at[1, d], x_r.at[1, d], across_x)
+
+    def kv_copy(i, d):
+        src, dst = stream[i]
+        block = lax.rem(z - d + groups, groups) * 2 + y
+        return remote(
+            src if d == 0 else dst.at[block], dst.at[block], kvy_s.at[i, d], kvy_r.at[i, d], across_y
+        )
+
+    @pl.when(y == 0)
+    def _():
+        for i in range(3):
+            kv_copy(i, 0).start()
+
+    y_copy(0).start()
+    x_copy(0).start()
+    weights = [
+        remote(src, dst, w_s.at[i], w_r.at[i], across_c)
+        for i, (src, dst) in enumerate(((gate, gate_o), (up, up_o), (down, down_o)))
+    ]
+    for copy in weights:
+        copy.start()
+    locals_ = [
+        pltpu.make_async_copy(src, dst.at[ep], local_sem.at[i])
+        for i, (src, dst) in enumerate(stream)
+    ] + [pltpu.make_async_copy(slots.at[z], rows.at[own, z], local_sem.at[3])]
+    for copy in locals_:
+        copy.start()
+
+    for d in range(1, groups):
+        @pl.when(z >= d)
+        def _(d=d):
+            for i, (src, dst) in enumerate(stream):
+                remote(src, dst.at[ep], kvz_s.at[i, d], kvz_r.at[i, d], across_y).wait_recv()
+                kv_copy(i, d).start()
+
+        y_copy(d - 1).wait_recv()
+        x_relay(d - 1).start()
+        z_copy(d).wait_recv()
+        y_copy(d).start()
+        x_copy(d).start()
+    y_copy(groups - 1).wait_recv()
+    x_relay(groups - 1).start()
+
+    for copy in locals_:
+        copy.wait()
+    for copy in weights:
+        copy.wait()
+    for i in range(3):
+        @pl.when(y == 1)
+        def _(i=i):
+            kv_copy(i, 0).wait_recv()
+
+        @pl.when(y == 0)
+        def _(i=i):
+            kv_copy(i, 0).wait_send()
+
+        for d in range(1, groups):
+            @pl.when(z >= d)
+            def _(i=i, d=d):
+                kv_copy(i, d).wait()
+
+            @pl.when(z + d < groups)
+            def _(i=i, d=d):
+                src, dst = stream[i]
+                remote(src, dst.at[ep], kvz_s.at[i, d], kvz_r.at[i, d], across_y).wait_send()
+
+    for d in range(groups):
+        if d:
+            z_copy(d).wait_send()
+        y_copy(d).wait_send()
+        x_copy(d).wait()
+        x_relay(d).wait()
+
+
+def dispatch(slots, keys, vals, cum, gate, up, down, ep_count):
+    groups, cap, width = slots.shape
+    dma = pltpu.SemaphoreType.DMA
+    like = lambda a: jax.ShapeDtypeStruct(a.shape, a.dtype)
+    many = lambda a: jax.ShapeDtypeStruct((ep_count,) + a.shape, a.dtype)
+    return pl.pallas_call(
+        functools.partial(dispatch_kernel, groups),
+        name="dispatch",
+        out_shape=(
+            jax.ShapeDtypeStruct((4, groups, cap, width), slots.dtype),
+            many(keys), many(vals), many(cum), like(gate), like(up), like(down),
+        ),
+        in_specs=[VMEM] * 4 + [ANY] * 3,
+        out_specs=(ANY,) * 7,
+        scratch_shapes=[
+            dma((4,)), dma((3, groups)), dma((3, groups)), dma((3, groups)), dma((3, groups)),
+            dma((3,)), dma((3,)), dma((groups,)), dma((groups,)), dma((groups,)), dma((groups,)),
+            dma((2, groups)), dma((2, groups)),
+        ],
+        compiler_params=pltpu.CompilerParams(
+            collective_id=0, has_side_effects=True, vmem_limit_bytes=8 * 1024 * 1024
+        ),
+    )(slots, keys, vals, cum, gate, up, down)
+
+
+def collect_kernel(
+    groups, part, mix, ret, mixed,
+    xr, ysum, yr, zsum, mr, msum, mx,
+    local_sem, x_s, x_r, y_s, y_r, z_s, z_r, c_s, c_r, m_s, m_r,
+):
+    ep, tp, z, y, x, c = places()
+    greet(groups)
+    across_y = (z * 2 + 1 - y, tp)
+    across_x = (ep, (1 - x) * 2 + c)
+    across_c = (ep, x * 2 + 1 - c)
+
+    def to_of(d):
+        return lax.rem(z + d, groups)
+
+    def c_copy(i):
+        return remote(mix.at[i, 1 - c], mr.at[i], c_s.at[i], c_r.at[i], across_c)
+
+    def x_copy(i, d):
+        column = 1 - y if i == 0 else y
+        return remote(
+            part.at[1 - x, column, to_of(d)], xr.at[i, d], x_s.at[i, d], x_r.at[i, d], across_x
+        )
+
+    def y_copy(d):
+        return remote(ysum.at[d], yr.at[d], y_s.at[d], y_r.at[d], across_y)
+
+    def z_copy(d):
+        return remote(zsum.at[d], ret.at[z], z_s.at[d], z_r.at[d], (to_of(d) * 2 + y, tp))
+
+    m_copy = remote(msum, mx, m_s, m_r, across_x)
+    local = pltpu.make_async_copy(zsum.at[0], ret.at[z], local_sem)
+    order = list(range(1, groups)) + [0]
+    for i in range(2):
+        c_copy(i).start()
+    for d in order:
+        x_copy(0, d).start()
+        x_copy(1, d).start()
+    for i in range(2):
+        c_copy(i).wait_recv()
+    f32 = jnp.float32
+    msum[...] = (mix[1 - x, c].astype(f32) + mr[1 - x].astype(f32)).astype(msum.dtype)
+    m_copy.start()
+    for step, d in enumerate(order):
+        x_copy(0, d).wait_recv()
+        ysum[d] = (part[x, 1 - y, to_of(d)].astype(f32) + xr[0, d].astype(f32)).astype(ysum.dtype)
+        y_copy(d).start()
+        for last in ([order[step - 1]] if step else []) + ([d] if step == groups - 1 else []):
+            x_copy(1, last).wait_recv()
+            y_copy(last).wait_recv()
+            zsum[last] = (
+                part[x, y, to_of(last)].astype(f32) + xr[1, last].astype(f32) + yr[last].astype(f32)
+            ).astype(zsum.dtype)
+            if last:
+                z_copy(last).start()
+            else:
+                local.start()
+    m_copy.wait_recv()
+    mixed[...] = mix[x, c].astype(f32) + mr[x].astype(f32) + mx[...].astype(f32)
+    local.wait()
+    m_copy.wait_send()
+    for i in range(2):
+        c_copy(i).wait_send()
+    for d in range(groups):
+        x_copy(0, d).wait_send()
+        x_copy(1, d).wait_send()
+        y_copy(d).wait_send()
+        if d:
+            z_copy(d).wait()
+
+
+def collect(part, mix):
+    groups, cap, width = part.shape[2:]
+    own = mix.shape[2]
+    dma = pltpu.SemaphoreType.DMA
+    bf16 = jnp.bfloat16
+    return pl.pallas_call(
+        functools.partial(collect_kernel, groups),
+        name="collect",
+        out_shape=(
+            jax.ShapeDtypeStruct((groups, cap, width), bf16),
+            jax.ShapeDtypeStruct((own, width), jnp.float32),
+        ),
+        in_specs=[VMEM] * 2,
+        out_specs=(VMEM,) * 2,
+        scratch_shapes=[
+            pltpu.VMEM((2, groups, cap, width), bf16),
+            pltpu.VMEM((groups, cap, width), bf16),
+            pltpu.VMEM((groups, cap, width), bf16),
+            pltpu.VMEM((groups, cap, width), bf16),
+            pltpu.VMEM((2, own, width), bf16),
+            pltpu.VMEM((own, width), bf16),
+            pltpu.VMEM((own, width), bf16),
+            dma, dma((2, groups)), dma((2, groups)), dma((groups,)), dma((groups,)),
+            dma((groups,)), dma((groups,)), dma((2,)), dma((2,)), dma, dma,
+        ],
+        compiler_params=pltpu.CompilerParams(
+            collective_id=1, has_side_effects=True, vmem_limit_bytes=40 * 1024 * 1024
+        ),
+    )(part, mix)
+
+
+def attend_kernel(ratio, tile, place, q_ref, k_ref, v_ref, cum_ref, qcum_ref, w_ref, out_ref):
+    ep = place[0]
+    rows, heads = qcum_ref.shape
+    f32 = jnp.float32
+    nt = (((1,), (1,)), ((), ()))
+    for start in range(0, rows, tile):
+        done = []
+        for h in range(heads):
+            head = slice((h // ratio) * DH, (h // ratio + 1) * DH)
+            q = q_ref[start : start + tile, h * DH : (h + 1) * DH]
+            qcum = qcum_ref[start : start + tile, h : h + 1] * LOG2E
+            width = start + tile
+
+            def weigh(s, bias, block, length):
+                v = v_ref[block, :length, head]
+                return jnp.dot(s.astype(jnp.bfloat16), v, preferred_element_type=f32)
+
+            s = lax.dot_general(q, k_ref[ep, :width, head], nt, preferred_element_type=f32)
+            s = s * (LOG2E / math.sqrt(DH)) + (qcum - cum_ref[ep, h : h + 1, :width] * LOG2E)
+            r = lax.broadcasted_iota(jnp.int32, s.shape, 0) + start
+            k = lax.broadcasted_iota(jnp.int32, s.shape, 1)
+            s = jnp.where(k <= r, s, -1e30)
+            top = jnp.max(s, axis=1, keepdims=True)
+            e = jnp.exp2(s - top)
+            total = jnp.sum(e, axis=1, keepdims=True)
+            acc = weigh(e, None, ep, width)
+
+            def step(i, state):
+                top, total, acc, gap = state
+                j = ep - 1 - i
+                gap = gap + cum_ref[j, h : h + 1, rows - 1 : rows] * LOG2E
+                s = lax.dot_general(q, k_ref[j, :, head], nt, preferred_element_type=f32)
+                s = s * (LOG2E / math.sqrt(DH)) + (
+                    qcum + (gap - cum_ref[j, h : h + 1, :] * LOG2E)
+                )
+                new = jnp.maximum(top, jnp.max(s, axis=1, keepdims=True))
+                e = jnp.exp2(s - new)
+                scale = jnp.exp2(top - new)
+                total = total * scale + jnp.sum(e, axis=1, keepdims=True)
+                return new, total, acc * scale + weigh(e, None, j, rows), gap
+
+            top, total, acc, _ = lax.fori_loop(
+                0, ep, step, (top, total, acc, jnp.zeros((1, 1), f32))
+            )
+            done.append((acc / total).astype(jnp.bfloat16))
+        attended = jnp.concatenate(done, axis=1)
+        out_ref[start : start + tile, :] = jnp.dot(
+            attended, w_ref[...], preferred_element_type=f32
+        ).astype(out_ref.dtype)
+
+
+def attend(place, queries, keys_all, vals_all, cum_all, qcum, out_weight, ratio):
+    rows = queries.shape[0]
+    return pl.pallas_call(
+        functools.partial(attend_kernel, ratio, math.gcd(rows, 256)),
+        name="attend",
+        out_shape=jax.ShapeDtypeStruct((rows, out_weight.shape[1]), jnp.bfloat16),
+        in_specs=[pl.BlockSpec(memory_space=pltpu.SMEM)] + [VMEM] * 6,
+        out_specs=VMEM,
+        compiler_params=pltpu.CompilerParams(vmem_limit_bytes=40 * 1024 * 1024),
+    )(place, queries, keys_all, vals_all, cum_all, qcum, out_weight)
+
+
+def expert_kernel(place, rows, gate, gate_o, up, up_o, down, down_o, router, out):
+    expert = place[0]
+    group = expert // 2
+    f32 = jnp.float32
+    block = rows[...]
+    dot = lambda a, b: jnp.dot(a, b[...], preferred_element_type=f32)
+    logits = dot(block, router)
+    lane = lax.broadcasted_iota(jnp.int32, logits.shape, 1)
+    pick = lambda index: jnp.sum(jnp.where(lane == index, logits, 0.0), axis=1, keepdims=True)
+    in_group = lane < GROUPS
+    top = jnp.max(jnp.where(in_group, logits, -jnp.inf), axis=1, keepdims=True)
+    total = jnp.sum(jnp.where(in_group, jnp.exp(logits - top), 0.0), axis=1, keepdims=True)
+    other = expert + 1 - 2 * (expert % 2)
+    share = jnp.exp(pick(group) - top) / total
+    share = share * jax.nn.sigmoid(pick(GROUPS + expert) - pick(GROUPS + other))
+    result = None
+    for g, u, w in ((gate, up, down), (gate_o, up_o, down_o)):
+        hidden = (jax.nn.silu(dot(block, g)) * dot(block, u)).astype(jnp.bfloat16)
+        term = dot(hidden, w)
+        result = term if result is None else result + term
+    out[...] = (share * result).astype(out.dtype)
+
+
+def run_experts(place, rows, gate, gate_o, up, up_o, down, down_o, router):
+    count, width = rows.shape
+    tile = math.gcd(count, 256)
+    full = lambda a: pl.BlockSpec(a.shape, lambda i: (0, 0), pipeline_mode=pl.Buffered(1))
+    return pl.pallas_call(
+        expert_kernel,
+        name="experts",
+        grid=(count // tile,),
+        out_shape=jax.ShapeDtypeStruct((count, width), jnp.bfloat16),
+        in_specs=[
+            pl.BlockSpec(memory_space=pltpu.SMEM),
+            pl.BlockSpec((tile, width), lambda i: (i, 0)),
+        ]
+        + [full(a) for a in (gate, gate_o, up, up_o, down, down_o, router)],
+        out_specs=pl.BlockSpec((tile, width), lambda i: (i, 0)),
+        compiler_params=pltpu.CompilerParams(vmem_limit_bytes=48 * 1024 * 1024),
+    )(place, rows, gate, gate_o, up, up_o, down, down_o, router)
+
+
+def paired_body(
+    queries, key_rows, value_rows, forget_logit, out_weight, out_gain, moe_input, moe_gain,
+    router_group, router_expert, route_group, route_pick, expert_gate, expert_up, expert_down,
+):
+    tp_count = lax.axis_size("tp")
+    ep_count = lax.axis_size("ep")
+    tp_index = lax.axis_index("tp")
+    place = lax.axis_index("ep").reshape(1).astype(jnp.int32)
+    own_rows = moe_input.shape[0] // tp_count
+    width = moe_input.shape[1]
+    experts = expert_gate.shape[0] * ep_count
+    capacity = tp_count * own_rows // experts
+    ratio = forget_logit.shape[0] // (key_rows.shape[1] // DH)
+    first = tp_index * own_rows
+    local_cum = jnp.cumsum(jax.nn.log_sigmoid(forget_logit), axis=1)
+    group = lax.dynamic_slice_in_dim(route_group, first, own_rows, 0)
+    normed = rms_scale(
+        lax.dynamic_slice_in_dim(moe_input, first, own_rows, 0), moe_gain
+    ).astype(jnp.bfloat16)
+    index = jnp.arange(own_rows, dtype=jnp.int32)
+    earlier = (group[:, None] == group[None, :]) & (index[:, None] < index[None, :])
+    rank = jnp.sum(earlier.astype(jnp.int32), axis=0)
+    slot = jnp.where(rank < capacity, group * capacity + rank, -1)
+    hot = (jnp.arange(GROUPS * capacity, dtype=jnp.int32)[:, None] == slot[None, :]).astype(
+        jnp.bfloat16
+    )
+    slots = jnp.dot(hot, normed, preferred_element_type=jnp.float32).astype(jnp.bfloat16)
+    rows, keys_all, vals_all, cum_all, gate_o, up_o, down_o = dispatch(
+        slots.reshape(GROUPS, capacity, width), key_rows, value_rows, local_cum,
+        expert_gate[0], expert_up[0], expert_down[0], ep_count,
+    )
+    mix = attend(place, queries, keys_all, vals_all, cum_all, local_cum.T, out_weight, ratio)
+    router = jnp.concatenate([router_group, router_expert], axis=1)
+    router = jnp.pad(router, ((0, 0), (0, -router.shape[1] % 128)))
+    part = run_experts(
+        place, rows.reshape(-1, width), expert_gate[0], gate_o, expert_up[0], up_o,
+        expert_down[0], down_o, router,
+    )
+    returned, mixed = collect(
+        part.reshape(2, 2, GROUPS, capacity, width), mix.reshape(2, 2, own_rows, width)
+    )
+    mixer_out = rms_scale(mixed, out_gain).astype(jnp.bfloat16)
+    moe_out = lax.dot_general(
+        hot, returned.reshape(-1, width), (((0,), (0,)), ((), ())),
+        preferred_element_type=jnp.float32,
+    )
+    return (mixer_out, moe_out.astype(jnp.bfloat16))
+
+
+def body(*args):
+    experts = args[12].shape[0] * lax.axis_size("ep")
+    if experts == 2 * GROUPS and args[12].shape[0] == 1 and lax.axis_size("tp") == 4:
+        return paired_body(*args)
+    return general_body(*args)
+
+
 def solution(mesh):
     in_specs = (
         P("ep", "tp"),

time: 392 us -> 198 us (0.51)
  waiting for transfers between devices: 170 us -> 0 us
  Pallas kernels: 0 us -> 161 us
  blocking collectives: 107 us -> 0 us
  matrix products: 29.6 us -> 3.7 us
  starting transfers between devices: 23.9 us -> 0 us
  between operations: 14 us -> 0.8 us
  other arithmetic: 16.1 us -> 4.13 us
  loops' own time: 5.77 us -> 0 us
    pallas_call x0 -> x4, Pallas kernels: none -> 161 us  [the longest x1 92.6 us: collect(): pl.pallas_call(functools.partial(collect_kernel, groups), name='collect',...]
    all_gather x3 -> x0, waiting for transfers between devices: 79.2 us -> none  [the longest x1 55.9 us: body(): hidden_arrived = lax.all_gather(arrived[None], 'tp', axis=0, tiled=True)]
    reduce_scatter x2 -> x0, waiting for transfers between devices: 72.7 us -> none  [the longest x1 46.7 us: body(): lax.psum_scatter(expert_term.astype(jnp.bfloat16), 'tp', scatter_dimensio...]
    all_to_all x1 -> x0, blocking collectives: 55.6 us -> none  [body(): lax.all_to_all(outgoing, 'ep', split_axis=0, concat_axis=0, tiled=True)]
    all_gather x1 -> x0, blocking collectives: 51.7 us -> none  [body(): lax.all_gather(local_cum, 'ep', axis=1, tiled=True)]
    dot_general x7 -> x2, matrix products: 29.6 us -> 3.7 us  [the longest x1 2.55 us: paired_body(): jnp.dot(hot, normed, preferred_element_type=jnp.float32)]
    all_to_all x1 -> x0, starting transfers between devices: 23.7 us -> none  [body(): lax.all_to_all(results, 'ep', split_axis=0, concat_axis=0, tiled=True)]
    unnamed x17 -> x54, local copies, waits for them, and re-layouts: 0.83 us -> 23.4 us
  transfers between devices with their start and end apart: 6 -> 0, of which waited for: 5 -> 0; matrix products, arithmetic and copies ran while one was open for 12% -> 0% of each run, Pallas kernels for 0% -> 0%
where the time goes in v1:
time: 198 us; the launch traced here: 196 us
  Pallas kernels  161 us (81%)
  local copies, waits for them, and re-layouts  27 us (14%)
  other arithmetic  4.13 us (2%)
  matrix products  3.7 us (2%)
    pallas_call x1, Pallas kernels, collect(): pl.pallas_call(functools.partial(collect_kernel, groups), name='collect',...  92.6 us
    pallas_call x1, Pallas kernels, dispatch(): pl.pallas_call(functools.partial(dispatch_kernel, groups), name='dispatch...  54.1 us
    unnamed x54, local copies, waits for them, and re-layouts  23.4 us
    pallas_call x1, Pallas kernels, run_experts(): pl.pallas_call(expert_kernel, name='experts', grid=(count // tile,), out_...  11.2 us

profile of v1, /device:TPU:0, one launch (start us, length us, event | category | flops | bytes accessed | tf_op | source)
XLA Modules:
  0.0 196.2 jit_solution(18442975182160637485)
XLA Ops:
  0.6 0.0 copy-start.26
  0.6 0.0 copy-start.2
  0.7 0.0 copy-start.3
  0.7 0.0 copy-start.19
  0.7 0.9 dynamic_slice.6
  1.6 0.1 convert_reduce_fusion
  1.7 0.8 compare_select_fusion.1
  2.4 1.2 fusion
  3.7 2.5 %convolution_convert_fusion = bf16[256,2048]{1,0:T(8,128)(2,1)} fusion(f32[2048]{0:T(1024)} %param.22, f32[128]{0:T(128)S(1)} %add_rsqrt_fusion.1, bf16[512,2048]{1,0:T(8,128)(2,1)} %param.21, s32[]{:T(128)S(6)} %select_n.13, s32[128]{0:T(128)S(1)} %compare_select_fusion.1), kind=kOutput, calls=%fused_computation | convolution fusion | flops 135823360 | bytes 1582084 | tf_op jit(solution)/shard_map/dot_general | solution.py:606
  6.2 0.0 copy-done.26
  6.3 0.6 reduce-window.6
  6.9 0.2 slice_reduce_fusion
  7.1 0.2 reduce-window.9
  7.2 0.1 broadcast_add_fusion
  7.3 0.2 copy.27
  7.5 0.1 copy.28.cum
  7.6 0.0 copy-done.2
  7.6 0.0 copy-done.3
  7.6 0.0 copy-done.19
  7.6 0.0 copy-start.5
  7.6 1.2 copy-done.5
  8.8 0.0 copy-start.7
  8.8 1.2 copy-done.7
  10.1 0.0 copy-start.20
  10.1 0.9 copy-done.20
  11.0 54.1 %dispatch.1 = (bf16[4,4,64,2048]{3,2,1,0:T(8,128)(2,1)S(1)}, bf16[8,512,128]{2,1,0:T(8,128)(2,1)S(1)}, bf16[8,512,128]{2,1,0:T(8,128)(2,1)S(1)}, f32[8,2,512]{2,...) custom-call(bf16[4,64,2048]{2,1,0:T(8,128)(2,1)S(1)} %bitcast.23, ...), custom_call_target="tpu_custom_call" | custom-call | tf_op jit(solution)/shard_map/dispatch/pallas_call | solution.py:354
  65.0 0.0 copy-start.1
  65.0 1.9 copy-done.1
  67.0 0.0 copy-start.8
  67.0 1.0 copy-done.8
  68.0 0.0 copy-start.10
  68.0 1.0 copy-done.10
  69.0 0.0 copy-start.12
  69.0 1.1 copy-done.12
  70.0 0.0 copy-start.14
  70.0 1.0 copy-done.14
  71.0 0.0 copy-start.16
  71.0 1.0 copy-done.16
  72.0 0.0 copy-start.21
  72.0 0.6 copy-done.21
  72.7 1.2 copy-done.13
  73.9 0.0 copy-start.15
  73.9 1.2 copy-done.15
  75.1 1.2 copy-done.17
  76.3 0.9 copy-done.18
  77.3 0.8 copy-done.22
  78.0 2.7 %attend.1 = bf16[512,2048]{1,0:T(8,128)(2,1)S(1)} custom-call(s32[1]{0:T(128)} %bitcast.place, bf16[512,256]{1,0:T(8,128)(2,1)S(1)} %copy-done.18, bf16[8,512,128]{2,1,0:T(8,128)(2,1)S(1)} %copy-done.15, bf16[8,512,128]{2,1,0:T(8,128)(2,1)S(1)} %copy-done.17, f32[8,2,512]{2,1,0:T(2,128)S(1)} %copy-done.22, f32[512,2]{1,0:T(8,128)S(1)} %bitcast.25, ...), custom_call_target="tpu_custom_call" | custom-call | tf_op jit(solution)/shard_map/attend/pallas_call | solution.py:528
  80.7 0.0 copy-done.23
  80.7 0.0 copy-done.24
  80.8 1.0 copy.29
  81.8 1.1 pad.4.router
  83.0 0.0 copy-start.4
  83.0 1.2 copy-done.4
  84.2 1.2 copy-done.6
  85.4 1.2 copy-done.9
  86.6 1.2 copy-done.11
  87.9 11.2 %experts.1 = bf16[1024,2048]{1,0:T(8,128)(2,1)} custom-call(s32[1]{0:T(128)} %bitcast.place, bf16[1024,2048]{1,0:T(8,128)(2,1)} %bitcast.16, bf16[2048,256]{1,0:T(8,128)(2,1)S(1)} %bitcast.18, bf16[2048,256]{1,0:T(8,128)(2,1)S(1)} %copy-done.9, bf16[2048,256]{1,0:T(8,128)(2,1)S(1)} %bitcast.20, bf16[2048,256]{1,0:T(8,128)(2,1)S(1)} %copy-done.11, ...), custom_call_target="tpu_custom_call" | custom-call | tf_op jit(solution)/shard_map/experts/pallas_call | solution.py:565
  99.1 2.2 %copy-done = bf16[1024,2048]{1,0:T(8,128)(2,1)S(1)} copy-done((bf16[1024,2048]{1,0:T(8,128)(2,1)S(1)}, bf16[1024,2048]{1,0:T(8,128)(2,1)}, u32[]{:S(2)}) %copy-start) | copy-done | bytes 4194328
  101.3 92.6 %collect.1 = (bf16[4,64,2048]{2,1,0:T(8,128)(2,1)S(1)}, f32[128,2048]{1,0:T(8,128)S(1)}) custom-call(bf16[2,2,4,64,2048]{4,3,2,1,0:T(8,128)(2,1)S(1)} %bitcast.14, bf16[2,2,128,2048]{3,2,1,0:T(8,128)(2,1)S(1)} %bitcast.15), custom_call_target="tpu_custom_call" | custom-call | tf_op jit(solution)/shard_map/collect/pallas_call | solution.py:449
  193.9 0.0 copy-start.25
  193.9 1.1 convolution_convert_fusion.1
  195.0 0.2 multiply_reduce_fusion
  195.2 0.0 copy-done.25
  195.2 1.0 multiply_convert_fusion
  (15 shorter events, 0.1 us)
Async XLA Ops:
  0.6 5.6 %copy-start.26 = (f32[2,512]{1,0:T(2,128)S(1)}, f32[2,512]{1,0:T(2,128)}, u32[]{:S(2)}) copy-start(f32[2,512]{1,0:T(2,128)} %param.18) | copy-start | bytes 12292
  0.6 6.9 %copy-start.2 = (bf16[1,2048,256]{2,1,0:T(8,128)(2,1)S(1)}, bf16[1,2048,256]{2,1,0:T(8,128)(2,1)}, u32[]{:S(2)}) copy-start(bf16[1,2048,256]{2,1,0:T(8,128)(2,1)} %param.26) | copy-start | bytes 3145732
  0.7 6.9 %copy-start.3 = (bf16[1,2048,256]{2,1,0:T(8,128)(2,1)S(1)}, bf16[1,2048,256]{2,1,0:T(8,128)(2,1)}, u32[]{:S(2)}) copy-start(bf16[1,2048,256]{2,1,0:T(8,128)(2,1)} %param.27) | copy-start | bytes 3145732
  0.7 6.9 %copy-start.19 = (bf16[512,128]{1,0:T(8,128)(2,1)S(1)}, bf16[512,128]{1,0:T(8,128)(2,1)}, u32[]{:S(2)}) copy-start(bf16[512,128]{1,0:T(8,128)(2,1)} %keys.1) | copy-start | bytes 393220
  7.6 1.2 copy-start.5
  8.8 1.2 copy-start.7
  10.1 0.9 copy-start.20
  65.0 2.0 copy-start.1
  67.0 1.0 copy-start.8
  68.0 1.0 copy-start.10
  69.0 1.1 copy-start.12
  70.0 1.0 copy-start.14
  71.0 1.0 copy-start.16
  72.0 0.6 copy-start.21
  72.7 1.2 copy-start.13
  73.9 1.2 copy-start.15
  75.1 1.2 copy-start.17
  76.3 0.9 copy-start.18
  77.3 0.8 copy-start.22
  78.0 2.7 %copy-start.23 = (bf16[2048,8]{0,1:T(8,128)(2,1)S(1)}, bf16[2048,8]{0,1:T(8,128)(2,1)}, u32[]{:S(2)}) copy-start(bf16[2048,8]{0,1:T(8,128)(2,1)} %param.24) | copy-start | bytes 98308
  78.0 2.7 %copy-start.24 = (bf16[2048,4]{0,1:T(4,128)(2,1)S(1)}, bf16[2048,4]{0,1:T(4,128)(2,1)}, u32[]{:S(2)}) copy-start(bf16[2048,4]{0,1:T(4,128)(2,1)} %param.23) | copy-start | bytes 49156
  83.0 1.2 copy-start.4
  84.2 1.2 copy-start.6
  85.4 1.2 copy-start.9
  86.6 1.2 copy-start.11
  99.1 2.2 %copy-start = (bf16[1024,2048]{1,0:T(8,128)(2,1)S(1)}, bf16[1024,2048]{1,0:T(8,128)(2,1)}, u32[]{:S(2)}) copy-start(bf16[1024,2048]{1,0:T(8,128)(2,1)} %experts.1) | copy-start | bytes 12582916
  193.9 1.3 copy-start.25

commit v2 on v0

--- a/solution.py
+++ b/solution.py
@@ -1,8 +1,11 @@
+import functools
 import math
 
 import jax
 import jax.numpy as jnp
 from jax import lax
+from jax.experimental import pallas as pl
+from jax.experimental.pallas import tpu as pltpu
 from jax.sharding import PartitionSpec as P
 
 DH = 128
@@ -33,7 +36,7 @@
     return hidden.reshape(arrived.shape[:-1] + (gate_part.shape[1],))
 
 
-def body(
+def general_body(
     queries,
     key_rows,
     value_rows,
@@ -199,6 +202,407 @@
     return (mixer_out, moe_out.astype(jnp.bfloat16))
 
 
+LOG2E = math.log2(math.e)
+MESH = pl.DeviceIdType.MESH
+VMEM = pl.BlockSpec(memory_space=pltpu.VMEM)
+ANY = pl.BlockSpec(memory_space=pl.ANY)
+
+
+def places():
+    ep, tp = lax.axis_index("ep"), lax.axis_index("tp")
+    return ep, tp, ep // 2, ep % 2, tp // 2, tp % 2
+
+
+def greet(groups):
+    ep, tp, z, y, x, c = places()
+    barrier = pltpu.get_barrier_semaphore()
+    peers = [(z * 2 + 1 - y, tp), (ep, (1 - x) * 2 + c), (ep, x * 2 + 1 - c)]
+    peers += [(lax.rem(z + d, groups) * 2 + y, tp) for d in range(1, groups)]
+    for peer in peers:
+        pl.semaphore_signal(barrier, inc=1, device_id=peer, device_id_type=MESH)
+    pl.semaphore_wait(barrier, len(peers))
+
+
+def remote(src, dst, send, recv, peer):
+    return pltpu.make_async_remote_copy(
+        src_ref=src, dst_ref=dst, send_sem=send, recv_sem=recv, device_id=peer, device_id_type=MESH
+    )
+
+
+def attend_tile(ratio, start, tile, ep, q_ref, k_ref, v_ref, cum_ref, qcum_ref):
+    rows, heads = qcum_ref.shape
+    f32 = jnp.float32
+    nt = (((1,), (1,)), ((), ()))
+    done = []
+    for h in range(heads):
+        head = slice((h // ratio) * DH, (h // ratio + 1) * DH)
+        q = q_ref[start : start + tile, h * DH : (h + 1) * DH]
+        qcum = qcum_ref[start : start + tile, h : h + 1] * LOG2E
+        width = start + tile
+        s = lax.dot_general(q, k_ref[ep, :width, head], nt, preferred_element_type=f32)
+        s = s * (LOG2E / math.sqrt(DH)) + (qcum - cum_ref[ep, h : h + 1, :width] * LOG2E)
+        r = lax.broadcasted_iota(jnp.int32, s.shape, 0) + start
+        k = lax.broadcasted_iota(jnp.int32, s.shape, 1)
+        s = jnp.where(k <= r, s, -1e30)
+        top = jnp.max(s, axis=1, keepdims=True)
+        e = jnp.exp2(s - top)
+        total = jnp.sum(e, axis=1, keepdims=True)
+        acc = jnp.dot(e.astype(jnp.bfloat16), v_ref[ep, :width, head], preferred_element_type=f32)
+
+        def step(i, state):
+            top, total, acc, gap = state
+            j = ep - 1 - i
+            gap = gap + cum_ref[j, h : h + 1, rows - 1 : rows] * LOG2E
+            s = lax.dot_general(q, k_ref[j, :, head], nt, preferred_element_type=f32)
+            s = s * (LOG2E / math.sqrt(DH)) + (qcum + (gap - cum_ref[j, h : h + 1, :] * LOG2E))
+            new = jnp.maximum(top, jnp.max(s, axis=1, keepdims=True))
+            e = jnp.exp2(s - new)
+            scale = jnp.exp2(top - new)
+            total = total * scale + jnp.sum(e, axis=1, keepdims=True)
+            acc = acc * scale + jnp.dot(
+                e.astype(jnp.bfloat16), v_ref[j, :, head], preferred_element_type=f32
+            )
+            return new, total, acc, gap
+
+        top, total, acc, _ = lax.fori_loop(0, ep, step, (top, total, acc, jnp.zeros((1, 1), f32)))
+        done.append((acc / total).astype(jnp.bfloat16))
+    return jnp.concatenate(done, axis=1)
+
+
+def expert_rows(expert, block, router, weights):
+    f32 = jnp.float32
+    group = expert // 2
+    dot = lambda a, b: jnp.dot(a, b[...], preferred_element_type=f32)
+    logits = lax.dot_general(
+        block, router[...], (((1,), (1,)), ((), ())), preferred_element_type=f32
+    )
+    lane = lax.broadcasted_iota(jnp.int32, logits.shape, 1)
+    pick = lambda index: jnp.sum(jnp.where(lane == index, logits, 0.0), axis=1, keepdims=True)
+    in_group = lane < GROUPS
+    top = jnp.max(jnp.where(in_group, logits, -jnp.inf), axis=1, keepdims=True)
+    total = jnp.sum(jnp.where(in_group, jnp.exp(logits - top), 0.0), axis=1, keepdims=True)
+    other = expert + 1 - 2 * (expert % 2)
+    share = jnp.exp(pick(group) - top) / total
+    share = share * jax.nn.sigmoid(pick(GROUPS + expert) - pick(GROUPS + other))
+    result = None
+    for g, u, w in weights:
+        hidden = (jax.nn.silu(dot(block, g)) * dot(block, u)).astype(jnp.bfloat16)
+        term = dot(hidden, w)
+        result = term if result is None else result + term
+    return (share * result).astype(jnp.bfloat16)
+
+
+def main_kernel(
+    groups, ratio,
+    slots, keys, vals, cum, gate, up, down, queries, out_weight, qcum, router,
+    ret, mixed,
+    rows, keys_all, vals_all, cum_all, gate_i, up_i, down_i, gate_o, up_o, down_o, q_v, w_v,
+    part, xr, ysum, yr, zsum, mix, mr, msum, mx,
+    local_sem, ret_sem, kvz_s, kvz_r, kvy_s, kvy_r, w_s, w_r, z_s, z_r, y_s, y_r, x_s, x_r, e_s, e_r,
+    bx_s, bx_r, by_s, by_r, bz_s, bz_r, c_s, c_r, m_s, m_r,
+):
+    ep, tp, z, y, x, c = places()
+    f32 = jnp.float32
+    greet(groups)
+    across_y = (z * 2 + 1 - y, tp)
+    across_x = (ep, (1 - x) * 2 + c)
+    across_c = (ep, x * 2 + 1 - c)
+    own = x * 2 + y
+    by_y = x * 2 + 1 - y
+    by_x = (1 - x) * 2 + y
+    stream = ((keys, keys_all), (vals, vals_all), (cum, cum_all))
+    far = lambda d: d % 2 == 1
+
+    def origin(d):
+        return lax.rem(z - d + groups, groups)
+
+    def z_copy(d):
+        to = lax.rem(z + d, groups)
+        return remote(slots.at[to], rows.at[z, own], z_s.at[d], z_r.at[d], (to * 2 + y, tp))
+
+    def piece(q, d):
+        return rows.at[origin(d), q]
+
+    def y_copy(d):
+        src = slots.at[z] if d == 0 else piece(own, d)
+        return remote(src, piece(own, d), y_s.at[d], y_r.at[d], across_y)
+
+    def x_copy(d):
+        src = slots.at[z] if d == 0 else piece(own, d)
+        return remote(src, piece(own, d), x_s.at[d], x_r.at[d], across_x)
+
+    def relay(d):
+        q, to = (by_x, across_y) if far(d) else (by_y, across_x)
+        return remote(piece(q, d), piece(q, d), e_s.at[d], e_r.at[d], to)
+
+    def kvz_copy(i, d):
+        src, dst = stream[i]
+        to = (lax.rem(z + d, groups) * 2 + y, tp)
+        return remote(src, dst.at[ep], kvz_s.at[i, d], kvz_r.at[i, d], to)
+
+    def kvy_copy(i, d):
+        src, dst = stream[i]
+        block = origin(d) * 2 + y
+        return remote(
+            src if d == 0 else dst.at[block], dst.at[block], kvy_s.at[i, d], kvy_r.at[i, d], across_y
+        )
+
+    def c_copy(i):
+        return remote(mix.at[i, 1 - c], mr.at[i], c_s.at[i], c_r.at[i], across_c)
+
+    def back_x(i, d):
+        q = (1 - x) * 2 + (1 - y if i == 0 else y)
+        return remote(piece_out(q, d), xr.at[i, d], bx_s.at[i, d], bx_r.at[i, d], across_x)
+
+    def piece_out(q, d):
+        return part.at[origin(d), q]
+
+    def back_y(d):
+        return remote(ysum.at[d], yr.at[d], by_s.at[d], by_r.at[d], across_y)
+
+    def back_z(d):
+        to = (origin(d) * 2 + y, tp)
+        return remote(zsum.at[d], ret.at[z], bz_s.at[d], bz_r.at[d], to)
+
+    y_copy(0).start()
+    x_copy(0).start()
+    z_copy(1).start()
+    for d in range(1, groups):
+        @pl.when(z + d < groups)
+        def _(d=d):
+            for i in range(3):
+                kvz_copy(i, d).start()
+
+    for d in range(2, groups):
+        z_copy(d).start()
+
+    @pl.when(y == 0)
+    def _():
+        for i in range(3):
+            kvy_copy(i, 0).start()
+
+    loads = (
+        (slots.at[z], piece(own, 0)), (gate, gate_i), (up, up_i), (down, down_i),
+        (keys, keys_all.at[ep]), (vals, vals_all.at[ep]), (cum, cum_all.at[ep]),
+        (queries, q_v), (out_weight, w_v),
+    )
+    loads = [pltpu.make_async_copy(src, dst, local_sem.at[i]) for i, (src, dst) in enumerate(loads)]
+    swaps = [
+        remote(src, dst, w_s.at[i], w_r.at[i], across_c)
+        for i, (src, dst) in enumerate(((gate, gate_o), (up, up_o), (down, down_o)))
+    ]
+    for copy in loads + swaps:
+        copy.start()
+
+    def pass_on(d):
+        z_copy(d).wait_recv()
+        y_copy(d).start()
+        x_copy(d).start()
+
+        @pl.when(z >= d)
+        def _():
+            for i in range(3):
+                kvz_copy(i, d).wait_recv()
+                kvy_copy(i, d).start()
+
+    def turn(d):
+        (x_copy(d) if far(d) else y_copy(d)).wait_recv()
+        relay(d).start()
+
+    def experts(d):
+        (y_copy(d) if far(d) else x_copy(d)).wait_recv()
+        relay(d).wait_recv()
+        at = origin(d)
+        block = rows[at].reshape(-1, rows.shape[-1])
+        out = expert_rows(ep, block, router, ((gate_i, up_i, down_i), (gate_o, up_o, down_o)))
+        part[at] = out.reshape(rows.shape[1:])
+        back_x(0, d).start()
+        back_x(1, d).start()
+
+    def fold_x(d):
+        back_x(0, d).wait_recv()
+        ysum[d] = (part[origin(d), by_y].astype(f32) + xr[0, d].astype(f32)).astype(ysum.dtype)
+        back_y(d).start()
+
+    home = pltpu.make_async_copy(zsum.at[0], ret.at[z], ret_sem)
+
+    def fold_y(d):
+        back_x(1, d).wait_recv()
+        back_y(d).wait_recv()
+        zsum[d] = (
+            part[origin(d), own].astype(f32) + xr[1, d].astype(f32) + yr[d].astype(f32)
+        ).astype(zsum.dtype)
+        if d:
+            back_z(d).start()
+        else:
+            home.start()
+
+    pass_on(1)
+    turn(0)
+    for copy in loads[:4] + swaps:
+        copy.wait()
+    experts(0)
+    pass_on(2)
+    turn(1)
+    experts(1)
+    pass_on(3)
+    turn(2)
+    fold_x(0)
+    turn(3)
+
+    for copy in loads[4:]:
+        copy.wait()
+    for i in range(3):
+        @pl.when(y == 1)
+        def _(i=i):
+            kvy_copy(i, 0).wait_recv()
+
+        @pl.when(y == 0)
+        def _(i=i):
+            kvy_copy(i, 0).wait_send()
+
+        for d in range(1, groups):
+            @pl.when(z >= d)
+            def _(i=i, d=d):
+                kvy_copy(i, d).wait()
+
+    experts(2)
+    length = qcum.shape[0]
+    tile = mix.shape[2]
+    for start in range(0, length, 2 * tile):
+        attended = attend_tile(
+            ratio, start, 2 * tile, ep, q_v, keys_all, vals_all, cum_all, qcum
+        )
+        out = jnp.dot(attended, w_v[...], preferred_element_type=f32).astype(mix.dtype)
+        mix[start // (2 * tile)] = out.reshape(mix.shape[1:])
+        c_copy(start // (2 * tile)).start()
+        if start == 0:
+            fold_x(1)
+            fold_y(0)
+    m_copy = remote(msum, mx, m_s, m_r, across_x)
+    experts(3)
+    for i in range(2):
+        c_copy(i).wait_recv()
+    msum[...] = (mix[1 - x, c].astype(f32) + mr[1 - x].astype(f32)).astype(msum.dtype)
+    m_copy.start()
+    fold_y(1)
+    fold_x(2)
+    fold_x(3)
+    fold_y(2)
+    fold_y(3)
+    m_copy.wait_recv()
+    mixed[...] = mix[x, c].astype(f32) + mr[x].astype(f32) + mx[...].astype(f32)
+
+    home.wait()
+    m_copy.wait_send()
+    for i in range(2):
+        c_copy(i).wait_send()
+    for d in range(groups):
+        y_copy(d).wait_send()
+        x_copy(d).wait_send()
+        relay(d).wait_send()
+        back_x(0, d).wait_send()
+        back_x(1, d).wait_send()
+        back_y(d).wait_send()
+        if d:
+            z_copy(d).wait_send()
+            back_z(d).wait()
+
+            @pl.when(z + d < groups)
+            def _(d=d):
+                for i in range(3):
+                    kvz_copy(i, d).wait_send()
+
+
+def run_main(slots, keys, vals, cum, gate, up, down, queries, out_weight, qcum, router, ep_count, ratio):
+    groups, cap, width = slots.shape
+    own = queries.shape[0] // 4
+    dma = pltpu.SemaphoreType.DMA
+    bf16 = jnp.bfloat16
+    same = lambda a: pltpu.VMEM(a.shape, a.dtype)
+    many = lambda a: pltpu.VMEM((ep_count,) + a.shape, a.dtype)
+    pieces = pltpu.VMEM((groups, cap, width), bf16)
+    tile = pltpu.VMEM((own, width), bf16)
+    line = dma((groups,))
+    return pl.pallas_call(
+        functools.partial(main_kernel, groups, ratio),
+        name="main",
+        out_shape=(
+            jax.ShapeDtypeStruct((groups, cap, width), bf16),
+            jax.ShapeDtypeStruct((own, width), jnp.float32),
+        ),
+        in_specs=[ANY] * 9 + [VMEM] * 2,
+        out_specs=(VMEM,) * 2,
+        scratch_shapes=[
+            pltpu.VMEM((groups, 4, cap, width), bf16),
+            many(keys), many(vals), many(cum),
+            same(gate), same(up), same(down), same(gate), same(up), same(down),
+            same(queries), same(out_weight),
+            pltpu.VMEM((groups, 4, cap, width), bf16),
+            pltpu.VMEM((2, groups, cap, width), bf16),
+            pieces, pieces, pieces,
+            pltpu.VMEM((2, 2, own, width), bf16),
+            pltpu.VMEM((2, own, width), bf16),
+            tile, tile,
+            dma((9,)), dma, dma((3, groups)), dma((3, groups)), dma((3, groups)), dma((3, groups)),
+            dma((3,)), dma((3,)), line, line, line, line, line, line, line, line,
+            dma((2, groups)), dma((2, groups)), line, line, line, line,
+            dma((2,)), dma((2,)), dma, dma,
+        ],
+        compiler_params=pltpu.CompilerParams(
+            collective_id=0, has_side_effects=True, vmem_limit_bytes=60 * 1024 * 1024
+        ),
+    )(slots, keys, vals, cum, gate, up, down, queries, out_weight, qcum, router)
+
+
+def paired_body(
+    queries, key_rows, value_rows, forget_logit, out_weight, out_gain, moe_input, moe_gain,
+    router_group, router_expert, route_group, route_pick, expert_gate, expert_up, expert_down,
+):
+    tp_count = lax.axis_size("tp")
+    ep_count = lax.axis_size("ep")
+    tp_index = lax.axis_index("tp")
+    own_rows = moe_input.shape[0] // tp_count
+    width = moe_input.shape[1]
+    experts = expert_gate.shape[0] * ep_count
+    capacity = tp_count * own_rows // experts
+    ratio = forget_logit.shape[0] // (key_rows.shape[1] // DH)
+    first = tp_index * own_rows
+    local_cum = jnp.cumsum(jax.nn.log_sigmoid(forget_logit), axis=1)
+    group = lax.dynamic_slice_in_dim(route_group, first, own_rows, 0)
+    normed = rms_scale(
+        lax.dynamic_slice_in_dim(moe_input, first, own_rows, 0), moe_gain
+    ).astype(jnp.bfloat16)
+    index = jnp.arange(own_rows, dtype=jnp.int32)
+    earlier = (group[:, None] == group[None, :]) & (index[:, None] < index[None, :])
+    rank = jnp.sum(earlier.astype(jnp.int32), axis=0)
+    slot = jnp.where(rank < capacity, group * capacity + rank, -1)
+    hot = (jnp.arange(GROUPS * capacity, dtype=jnp.int32)[:, None] == slot[None, :]).astype(
+        jnp.bfloat16
+    )
+    slots = jnp.dot(hot, normed, preferred_element_type=jnp.float32).astype(jnp.bfloat16)
+    router = jnp.concatenate([router_group.T, router_expert.T], axis=0)
+    router = jnp.pad(router, ((0, -router.shape[0] % 16), (0, 0)))
+    returned, mixed = run_main(
+        slots.reshape(GROUPS, capacity, width), key_rows, value_rows, local_cum,
+        expert_gate[0], expert_up[0], expert_down[0], queries, out_weight, local_cum.T, router,
+        ep_count, ratio,
+    )
+    mixer_out = rms_scale(mixed, out_gain).astype(jnp.bfloat16)
+    moe_out = lax.dot_general(
+        hot, returned.reshape(-1, width), (((0,), (0,)), ((), ())),
+        preferred_element_type=jnp.float32,
+    )
+    return (mixer_out, moe_out.astype(jnp.bfloat16))
+
+
+def body(*args):
+    experts = args[12].shape[0] * lax.axis_size("ep")
+    if experts == 2 * GROUPS and args[12].shape[0] == 1 and lax.axis_size("tp") == 4:
+        return paired_body(*args)
+    return general_body(*args)
+
+
 def solution(mesh):
     in_specs = (
         P("ep", "tp"),

time: 392 us -> 156 us (0.40)
  waiting for transfers between devices: 170 us -> 0 us
  Pallas kernels: 0 us -> 142 us
  blocking collectives: 107 us -> 0 us
  matrix products: 29.6 us -> 5.02 us
  starting transfers between devices: 23.9 us -> 0 us
  local copies, waits for them, and re-layouts: 23.7 us -> 1.8 us
  between operations: 14 us -> 0.69 us
  other arithmetic: 16.1 us -> 6.22 us
  loops' own time: 5.77 us -> 0 us
    pallas_call x0 -> x1, Pallas kernels: none -> 142 us  [run_main(): pl.pallas_call(functools.partial(main_kernel, groups, ratio), name='main'...]
    all_gather x3 -> x0, waiting for transfers between devices: 79.2 us -> none  [the longest x1 55.9 us: body(): hidden_arrived = lax.all_gather(arrived[None], 'tp', axis=0, tiled=True)]
    reduce_scatter x2 -> x0, waiting for transfers between devices: 72.7 us -> none  [the longest x1 46.7 us: body(): lax.psum_scatter(expert_term.astype(jnp.bfloat16), 'tp', scatter_dimensio...]
    all_to_all x1 -> x0, blocking collectives: 55.6 us -> none  [body(): lax.all_to_all(outgoing, 'ep', split_axis=0, concat_axis=0, tiled=True)]
    all_gather x1 -> x0, blocking collectives: 51.7 us -> none  [body(): lax.all_gather(local_cum, 'ep', axis=1, tiled=True)]
    dot_general x7 -> x2, matrix products: 29.6 us -> 5.02 us  [the longest x1 2.56 us: paired_body(): jnp.dot(hot, normed, preferred_element_type=jnp.float32)]
    all_to_all x1 -> x0, starting transfers between devices: 23.7 us -> none  [body(): lax.all_to_all(results, 'ep', split_axis=0, concat_axis=0, tiled=True)]
    all_to_all x1 -> x0, waiting for transfers between devices: 16.4 us -> none  [body(): lax.all_to_all(results, 'ep', split_axis=0, concat_axis=0, tiled=True)]
  transfers between devices with their start and end apart: 6 -> 0, of which waited for: 5 -> 0; matrix products, arithmetic and copies ran while one was open for 12% -> 0% of each run, Pallas kernels for 0% -> 0%
where the time goes in v2:
time: 156 us
  Pallas kernels  142 us (91%)
  other arithmetic  6.22 us (4%)
  matrix products  5.02 us (3%)
  local copies, waits for them, and re-layouts  1.8 us (1%)
    pallas_call x1, Pallas kernels, run_main(): pl.pallas_call(functools.partial(main_kernel, groups, ratio), name='main'...  142 us

profile of v2, /device:TPU:0, one launch (start us, length us, event | category | flops | bytes accessed | tf_op | source)
XLA Modules:
  0.0 155.9 jit_solution(18261192837966931006)
XLA Ops:
  0.6 1.2 fusion
  1.9 0.8 dynamic_slice.6
  2.6 0.1 convert_reduce_fusion
  2.7 0.8 compare_select_fusion.1
  3.5 0.7 fusion.13
  4.2 0.6 reduce-window.6
  4.8 0.2 slice_reduce_fusion
  5.0 0.2 reduce-window.9
  5.2 0.1 broadcast_add_fusion
  5.3 1.4 fusion.9.router
  6.7 0.1 copy.20
  6.8 0.0 copy-start.1
  6.8 0.7 copy.21.cum
  7.6 2.6 %convolution_convert_fusion = bf16[256,2048]{1,0:T(8,128)(2,1)} fusion(f32[2048]{0:T(1024)} %param.22, f32[128]{0:T(128)S(1)} %add_rsqrt_fusion.1, bf16[512,2048]{1,0:T(8,128)(2,1)} %param.21, s32[]{:T(128)S(6)} %select_n.13, s32[128]{0:T(128)S(1)} %compare_select_fusion.1), kind=kOutput, calls=%fused_computation | convolution fusion | flops 135823360 | bytes 1582084 | tf_op jit(solution)/shard_map/dot_general | solution.py:583
  10.1 0.0 copy-done.1
  10.1 142.1 %main.1 = (bf16[4,64,2048]{2,1,0:T(8,128)(2,1)}, f32[128,2048]{1,0:T(8,128)}) custom-call(bf16[4,64,2048]{2,1,0:T(8,128)(2,1)} %bitcast.12, bf16[512,128]{1,0:T(8,128)(2,1)} %keys.1, bf16[512,128]{1,0:T(8,128)(2,1)} %vals.1, f32[2,512]{1,0:T(2,128)} %copy.21.cum, bf16[2048,256]{1,0:T(8,128)(2,1)} %bitcast.16, bf16[2048,256]{1,0:T(8,128)(2,1)} %bitcast.17, ...), custom_call_target="tpu_custom_call" | custom-call | tf_op jit(solution)/shard_map/main/pallas_call | solution.py:527
  152.3 0.0 copy-start
  152.3 0.0 copy-start.2
  152.3 2.5 %convolution_convert_fusion.1 = bf16[128,2048]{1,0:T(8,128)(2,1)} fusion(bf16[256,2048]{1,0:T(8,128)(2,1)} %bitcast.15, s32[128]{0:T(128)S(1)} %compare_select_fusion.1), kind=kOutput, calls=%fused_computation.1 | convolution fusion | flops 134512640 | bytes 1573376 | tf_op jit(solution)/shard_map/dot_general | solution.py:592
  154.7 0.0 copy-done
  154.7 0.2 multiply_reduce_fusion
  154.9 0.0 copy-done.2
  154.9 1.0 multiply_convert_fusion
  (3 shorter events, 0.0 us)
Async XLA Ops:
  6.8 3.3 %copy-start.1 = (f32[2,4,128]{0,2,1:T(8,128)}, f32[2,4,128]{0,2,1:T(8,128)S(1)}, u32[]{:S(2)}) copy-start(f32[2,4,128]{0,2,1:T(8,128)S(1)} %copy.20) | copy-start | bytes 12292
  152.3 2.5 %copy-start = (f32[128,2048]{1,0:T(8,128)S(1)}, f32[128,2048]{1,0:T(8,128)}, u32[]{:S(2)}) copy-start(f32[128,2048]{1,0:T(8,128)} %get-tuple-element.4) | copy-start | bytes 3145732
  152.3 2.6 %copy-start.2 = (f32[2048]{0:T(1024)S(1)}, f32[2048]{0:T(1024)}, u32[]{:S(2)}) copy-start(f32[2048]{0:T(1024)} %param.20) | copy-start | bytes 24580
